TPU v7x, 32 devices: a whole 2x2x4 slice. The times are simulated.
32 devices in a mesh: kv: 16 (over z, y, x), tp: 2 (over core).
Axes of the slice: x: 2, y: 2, z: 4, core: 2. Of those that a mesh axis runs over, the one named last changes fastest.
Arguments:
- tokens: bfloat16 [64, 4, 2048], P('kv', None, 'tp'), may hold values from -6 to 6
- input_gain: float32 [2048], replicated, may hold values from 0.1 to 1.9
- gate_weight: bfloat16 [2048, 4096], P('kv', 'tp'), may hold values from -0.125 to 0.125
- value_weight: bfloat16 [2048, 4096], P('kv', 'tp'), may hold values from -0.125 to 0.125
- write_weight: bfloat16 [2048, 1024], P('kv', 'tp'), may hold values from -0.125 to 0.125
- read_weight: bfloat16 [2048, 1024], P('kv', 'tp'), may hold values from -0.125 to 0.125
- step_weight: bfloat16 [2048, 64], replicated, may hold values from -0.125 to 0.125
- conv_value: float32 [4, 4096], P(None, 'tp'), may hold values from -3 to 3
- conv_write: float32 [4, 1024], P(None, 'tp'), may hold values from -3 to 3
- conv_read: float32 [4, 1024], P(None, 'tp'), may hold values from -3 to 3
- step_bias: float32 [64], P('tp'), may hold values from -4 to -1
- decay_log: float32 [64], P('tp'), may hold values from 0 to 2.8
- skip_gain: float32 [64], P('tp'), may hold values from 0.5 to 1.5
- output_gain: float32 [4096], P('tp'), may hold values from 0.1 to 1.9
- out_weight: bfloat16 [4096, 2048], P('tp', 'kv'), may hold values from -0.09375 to 0.09375
- base_state: float32 [64, 64, 64, 128], P('kv', 'tp'), may hold values from -2 to 2
- past_value: bfloat16 [64, 7, 4096], P('kv', None, 'tp'), may hold values from -6 to 6
- past_write: bfloat16 [64, 7, 1024], P('kv', None, 'tp'), may hold values from -6 to 6
- past_read: bfloat16 [64, 7, 1024], P('kv', None, 'tp'), may hold values from -6 to 6
- past_step: bfloat16 [64, 4, 64], P('kv', None, 'tp'), may hold values from -4 to 4
- accepted: int32 [64], P('kv'), may hold values from 1 to 4
Outputs:
- mixed: bfloat16 [64, 4, 2048], P('kv', None, 'tp')
- root_state: float32 [64, 64, 64, 128], P('kv', 'tp')
- next_value: bfloat16 [64, 7, 4096], P('kv', None, 'tp')
- next_write: bfloat16 [64, 7, 1024], P('kv', None, 'tp')
- next_read: bfloat16 [64, 7, 1024], P('kv', None, 'tp')
- next_step: bfloat16 [64, 4, 64], P('kv', None, 'tp')
Inputs may be any that keep to these rules, and one draw needn't show every extreme that they name: Every entry of `accepted` is an integer from 1 to 4 (at least one of the last step's proposals is always accepted).
All inputs are finite; a program needn't handle non-finite values.
Results may differ from a plain program's by a relative error of at most 0.018.
Values may be sent and summed in bfloat16 or wider, within the bound.
A program may use at most 64 MiB of HBM per device.

v0:
```python
import jax
import jax.numpy as jnp
from jax import lax
from jax.sharding import PartitionSpec as P

STATE_DIM = 128
CONV_W = 4


EPSILON = 1e-06


def causal_conv(rows, kernel):
    width = kernel.shape[0]
    count = rows.shape[0] - width + 1
    total = kernel[0] * rows[0:count]
    for offset in range(1, width):
        total = total + kernel[offset] * rows[offset : offset + count]
    return total


def advance(
    past_x,
    past_b,
    past_c,
    past_dt,
    taken,
    state_zero,
    value_now,
    write_now,
    read_now,
    gate_now,
    step_now,
    conv_value,
    conv_write,
    conv_read,
    step_bias,
    decay_log,
    skip_gain,
    output_gain,
):
    highest = lax.Precision.HIGHEST
    proposals = value_now.shape[0]
    head_count = step_bias.shape[0]
    group_count = write_now.shape[1] // STATE_DIM
    per_group = head_count // group_count
    head_width = value_now.shape[1] // head_count
    rate = jnp.exp(decay_log)
    prev_x = jax.nn.silu(causal_conv(past_x.astype(jnp.float32), conv_value)).reshape(
        proposals, head_count, head_width
    )
    prev_b = jax.nn.silu(causal_conv(past_b.astype(jnp.float32), conv_write)).reshape(
        proposals, group_count, STATE_DIM
    )
    prev_b = jnp.repeat(prev_b, per_group, axis=1)
    prev_dt = jax.nn.softplus(past_dt.astype(jnp.float32) + step_bias)
    live = (jnp.arange(proposals, dtype=jnp.int32) < taken)[:, None]
    prev_log = jnp.where(live, -rate * prev_dt, jnp.zeros_like(prev_dt))
    total_log = jnp.sum(prev_log, axis=0)
    tail_log = total_log - jnp.cumsum(prev_log, axis=0)
    weight_now = jnp.where(live, jnp.exp(tail_log) * prev_dt, jnp.zeros_like(prev_dt))
    root = jnp.exp(total_log)[:, None, None] * state_zero + jnp.einsum(
        "sh,shp,shn->hpn", weight_now, prev_x, prev_b, precision=highest
    )
    window_x = jnp.concatenate(
        [lax.dynamic_slice_in_dim(past_x, taken, CONV_W - 1, 0), value_now], axis=0
    )
    window_b = jnp.concatenate(
        [lax.dynamic_slice_in_dim(past_b, taken, CONV_W - 1, 0), write_now], axis=0
    )
    window_c = jnp.concatenate(
        [lax.dynamic_slice_in_dim(past_c, taken, CONV_W - 1, 0), read_now], axis=0
    )
    cur_x = jax.nn.silu(causal_conv(window_x.astype(jnp.float32), conv_value)).reshape(
        proposals, head_count, head_width
    )
    cur_b = jax.nn.silu(causal_conv(window_b.astype(jnp.float32), conv_write)).reshape(
        proposals, group_count, STATE_DIM
    )
    cur_c = jax.nn.silu(causal_conv(window_c.astype(jnp.float32), conv_read)).reshape(
        proposals, group_count, STATE_DIM
    )
    cur_b = jnp.repeat(cur_b, per_group, axis=1)
    cur_c = jnp.repeat(cur_c, per_group, axis=1)
    cur_dt = jax.nn.softplus(step_now.astype(jnp.float32) + step_bias)
    logs = jnp.cumsum(-rate * cur_dt, axis=0)
    carried = jnp.einsum("thn,hpn->thp", cur_c, root, precision=highest) * jnp.exp(logs)[:, :, None]
    lower = (jnp.arange(proposals)[:, None] >= jnp.arange(proposals)[None, :])[:, :, None]
    diff = logs[:, None, :] - logs[None, :, :]
    decay = jnp.where(
        lower, jnp.exp(jnp.where(lower, diff, jnp.zeros_like(diff))), jnp.zeros_like(diff)
    )
    scores = (
        jnp.einsum("thn,shn->tsh", cur_c, cur_b, precision=highest) * decay * cur_dt[None, :, :]
    )
    inner = jnp.einsum("tsh,shp->thp", scores, cur_x, precision=highest)
    mixed = carried + inner + skip_gain[None, :, None] * cur_x
    gated = mixed.reshape(proposals, -1) * jax.nn.silu(gate_now.astype(jnp.float32))
    grouped = gated.reshape(proposals, group_count, -1)
    grouped = grouped * lax.rsqrt(jnp.mean(grouped * grouped, axis=-1, keepdims=True) + EPSILON)
    result = (grouped.reshape(proposals, -1) * output_gain).astype(jnp.bfloat16)
    return (result, root, window_x, window_b, window_c)


def on_device(
    tokens,
    input_gain,
    gate_weight,
    value_weight,
    write_weight,
    read_weight,
    step_weight,
    conv_value,
    conv_write,
    conv_read,
    step_bias,
    decay_log,
    skip_gain,
    output_gain,
    out_weight,
    base_state,
    past_value,
    past_write,
    past_read,
    past_step,
    accepted,
):
    whole = lax.all_gather(tokens, "tp", axis=2, tiled=True)
    seq_local, proposals, width = whole.shape
    rows = whole.astype(jnp.float32)
    normed = (
        rows * lax.rsqrt(jnp.mean(rows * rows, axis=-1, keepdims=True) + EPSILON) * input_gain
    ).astype(jnp.bfloat16)
    flat = normed.reshape(seq_local * proposals, width)
    token_count = flat.shape[0]
    head_count = step_bias.shape[0]
    own_step = lax.dynamic_slice_in_dim(
        step_weight, lax.axis_index("tp") * head_count, head_count, 1
    )
    step_now = jnp.dot(flat, own_step, preferred_element_type=jnp.float32).astype(jnp.bfloat16)
    slabs = (
        lax.all_to_all(gate_weight, "kv", split_axis=1, concat_axis=0, tiled=True),
        lax.all_to_all(value_weight, "kv", split_axis=1, concat_axis=0, tiled=True),
        lax.all_to_all(write_weight, "kv", split_axis=1, concat_axis=0, tiled=True),
        lax.all_to_all(read_weight, "kv", split_axis=1, concat_axis=0, tiled=True),
    )
    spans = [slab.shape[1] for slab in slabs]
    narrow = jnp.concatenate(slabs, axis=1)
    everyone = jnp.dot(
        lax.all_gather(flat, "kv", axis=0, tiled=True), narrow, preferred_element_type=jnp.float32
    ).astype(jnp.bfloat16)
    returned = lax.all_to_all(everyone, "kv", split_axis=0, concat_axis=1, tiled=True)
    ranks = lax.axis_size("kv")
    returned = returned.reshape(token_count, ranks, sum(spans))
    pieces_out = []
    offset = 0
    for span in spans:
        pieces_out.append(returned[:, :, offset : offset + span].reshape(token_count, ranks * span))
        offset = offset + span
    gate_now, value_now, write_now, read_now = pieces_out
    shaped = [
        item.reshape(seq_local, proposals, item.shape[1])
        for item in (value_now, write_now, read_now, gate_now, step_now)
    ]
    stepper = jax.vmap(advance, in_axes=(0,) * 11 + (None,) * 7)
    normal_out, root_state, next_value, next_write, next_read = stepper(
        past_value,
        past_write,
        past_read,
        past_step,
        accepted,
        base_state,
        shaped[0],
        shaped[1],
        shaped[2],
        shaped[3],
        shaped[4],
        conv_value,
        conv_write,
        conv_read,
        step_bias,
        decay_log,
        skip_gain,
        output_gain,
    )
    flat_y = normal_out.reshape(token_count, -1)
    partial_sum = jnp.dot(
        flat_y,
        lax.all_gather(out_weight, "kv", axis=1, tiled=True),
        preferred_element_type=jnp.float32,
    )
    summed = lax.psum_scatter(
        partial_sum.astype(jnp.bfloat16), "tp", scatter_dimension=1, tiled=True
    ).astype(jnp.float32)
    mixed = summed.astype(jnp.bfloat16).reshape(seq_local, proposals, summed.shape[1])
    return (mixed, root_state, next_value, next_write, next_read, shaped[4])


def solution(mesh):
    return jax.shard_map(
        on_device,
        mesh=mesh,
        in_specs=(
            P("kv", None, "tp"),
            P(),
            P("kv", "tp"),
            P("kv", "tp"),
            P("kv", "tp"),
            P("kv", "tp"),
            P(),
            P(None, "tp"),
            P(None, "tp"),
            P(None, "tp"),
            P("tp"),
            P("tp"),
            P("tp"),
            P("tp"),
            P("tp", "kv"),
            P("kv", "tp", None, None),
            P("kv", None, "tp"),
            P("kv", None, "tp"),
            P("kv", None, "tp"),
            P("kv", None, "tp"),
            P("kv"),
        ),
        out_specs=(
            P("kv", None, "tp"),
            P("kv", "tp", None, None),
            P("kv", None, "tp"),
            P("kv", None, "tp"),
            P("kv", None, "tp"),
            P("kv", None, "tp"),
        ),
        check_vma=False,
    )
```

profile of v0, /device:TPU:0, one launch (start us, length us, event | category | flops | bytes accessed | tf_op | source)
XLA Modules:
  0.0 240.1 jit_solution(14722465819496785952)
XLA Ops:
  7.3 2.3 all_gather.9
  9.8 0.8 fusion.18
  10.6 0.6 reshape.162
  11.3 0.7 all-gather.5.cloned.1.call-update
  12.0 1.7 copy.196
  13.7 8.2 %all-to-all-start.2 = ((bf16[128,16,32]{0,2,1:T(8,128)(2,1)}), bf16[128,16,32]{0,2,1:T(8,128)(2,1)S(1)}, u32[]{:S(2)}, u32[]{:S(2)}) async-start(bf16[128,16,32]{0,2,1:T(8,128)(2,1)} %bitcast.19), calls=%async_computation.2 | async-start | bytes 262144 | tf_op jit(solution)/shard_map/all_to_all | solution.py:144
  21.9 1.7 copy.198
  23.6 6.5 %all-to-all-done.2 = bf16[128,16,32]{0,2,1:T(8,128)(2,1)S(1)} async-done(((bf16[128,16,32]{0,2,1:T(8,128)(2,1)}), bf16[128,16,32]{0,2,1:T(8,128)(2,1)S(1)}, u32[]{:S(2)}, u32[]{:S(2)}) %all-to-all-start.2) | async-done | bytes 131104 | tf_op jit(solution)/shard_map/all_to_all | solution.py:144
  30.1 3.5 %all-to-all-start.3 = ((bf16[128,16,32]{0,2,1:T(8,128)(2,1)}), bf16[128,16,32]{0,2,1:T(8,128)(2,1)S(1)}, u32[]{:S(2)}, u32[]{:S(2)}) async-start(bf16[128,16,32]{0,2,1:T(8,128)(2,1)} %bitcast.22), calls=%async_computation.3 | async-start | bytes 262144 | tf_op jit(solution)/shard_map/all_to_all | solution.py:145
  33.6 2.0 copy.192
  35.6 5.7 %all-to-all-done.3 = bf16[128,16,32]{0,2,1:T(8,128)(2,1)S(1)} async-done(((bf16[128,16,32]{0,2,1:T(8,128)(2,1)}), bf16[128,16,32]{0,2,1:T(8,128)(2,1)S(1)}, u32[]{:S(2)}, u32[]{:S(2)}) %all-to-all-start.3) | async-done | bytes 131104 | tf_op jit(solution)/shard_map/all_to_all | solution.py:145
  41.4 3.6 %all-to-all-start = ((bf16[128,16,128]{0,2,1:T(8,128)(2,1)}), bf16[128,16,128]{0,2,1:T(8,128)(2,1)S(1)}, u32[]{:S(2)}, u32[]{:S(2)}) async-start(bf16[128,16,128]{0,2,1:T(8,128)(2,1)} %bitcast.13), calls=%async_computation | async-start | bytes 1048576 | tf_op jit(solution)/shard_map/all_to_all | solution.py:142
  45.0 1.0 copy.194
  46.3 13.3 %all-to-all-done = bf16[128,16,128]{0,2,1:T(8,128)(2,1)S(1)} async-done(((bf16[128,16,128]{0,2,1:T(8,128)(2,1)}), bf16[128,16,128]{0,2,1:T(8,128)(2,1)S(1)}, u32[]{:S(2)}, u32[]{:S(2)}) %all-to-all-start) | async-done | bytes 524320 | tf_op jit(solution)/shard_map/all_to_all | solution.py:142
  59.6 3.9 %all-to-all-start.1 = ((bf16[128,16,128]{0,2,1:T(8,128)(2,1)}), bf16[128,16,128]{0,2,1:T(8,128)(2,1)S(1)}, u32[]{:S(2)}, u32[]{:S(2)}) async-start(bf16[128,16,128]{0,2,1:T(8,128)(2,1)} %bitcast.16), calls=%async_computation.1 | async-start | bytes 1048576 | tf_op jit(solution)/shard_map/all_to_all | solution.py:143
  63.8 0.8 gather_fusion.1
  65.5 0.6 gather_fusion
  67.2 12.8 %all-to-all-done.1 = bf16[128,16,128]{0,2,1:T(8,128)(2,1)S(1)} async-done(((bf16[128,16,128]{0,2,1:T(8,128)(2,1)}), bf16[128,16,128]{0,2,1:T(8,128)(2,1)S(1)}, u32[]{:S(2)}, u32[]{:S(2)}) %all-to-all-start.1) | async-done | bytes 524320 | tf_op jit(solution)/shard_map/all_to_all | solution.py:143
  80.3 2.3 fusion.10
  82.7 0.8 copy.202
  83.5 4.8 %all-to-all-start.4 = ((bf16[16,16,320]{2,1,0:T(8,128)(2,1)}), bf16[16,16,320]{2,1,0:T(8,128)(2,1)S(1)}, u32[]{:S(2)}, u32[]{:S(2)}) async-start(bf16[16,16,320]{2,1,0:T(8,128)(2,1)} %bitcast.25), calls=%async_computation.4 | async-start | bytes 393216 | tf_op jit(solution)/shard_map/all_to_all | solution.py:152
  88.5 7.9 %all-to-all-done.4 = bf16[16,16,320]{2,1,0:T(8,128)(2,1)S(1)} async-done(((bf16[16,16,320]{2,1,0:T(8,128)(2,1)}), bf16[16,16,320]{2,1,0:T(8,128)(2,1)S(1)}, u32[]{:S(2)}, u32[]{:S(2)}) %all-to-all-start.4) | async-done | bytes 163872 | tf_op jit(solution)/shard_map/all_to_all | solution.py:152
  98.2 1.1 fusion.9
  99.3 1.3 fusion.14
  100.6 7.6 %multiply_add_fusion = f32[4,32,64,128]{3,2,1,0:T(8,128)S(1)} fusion(f32[4,32,64,128]{3,2,1,0:T(8,128)S(1)} %copy-done.2, f32[4,4,32,128]{3,1,2,0:T(4,128)S(1)} %bitcast.104, f32[4,32]{1,0:T(4,128)S(1)} %exp.62, f32[4,4,32,64]{3,2,1,0:T(8,128)S(1)} %reshape.159, f32[4,4,32]{1,2,0:T(8,128)S(1)} %copy.187), kind=kOutput, calls=%fused_computation.3 | convolution fusion | flops 52461568 | bytes 8784384 | tf_op jit(solution)/shard_map/vmap(sh,shp,shn->hpn)/dot_general | solution.py:62
  108.2 2.0 copy-done.1
  110.2 6.8 %fusion.67 = f32[4,32,64,4]{2,3,1,0:T(4,128)S(1)} fusion(f32[4,32,64,128]{3,2,1,0:T(8,128)S(1)} %multiply_add_fusion, f32[4,4,32,128]{3,1,2,0:T(4,128)S(1)} %bitcast.103), kind=kOutput, calls=%fused_computation.121 | convolution fusion | flops 50331648 | bytes 4587520 | tf_op jit(solution)/shard_map/vmap(thn,hpn->thp)/dot_general | solution.py:87
  117.9 103.2 %all-gather.5.cloned.1.call-done = bf16[2048,2048]{1,0:T(8,128)(2,1)} async-done(((bf16[2048,128]{1,0:T(8,128)(2,1)}), bf16[2048,2048]{1,0:T(8,128)(2,1)}) %all-gather.5.cloned.1.call-update) | async-done | bytes 8388624 | tf_op jit(solution)/shard_map/all_gather | solution.py:189
  221.0 5.2 %convolution_convert_fusion = bf16[16,2048]{1,0:T(8,128)(2,1)} fusion(bf16[2048,2048]{1,0:T(8,128)(2,1)} %all-gather.5.cloned.1.call-done, f32[16,2048]{1,0:T(8,128)S(1)} %bitcast.105, f32[16,2048]{1,0:T(8,128)S(1)} %reshape.169, f32[16,2,8,128]{3,2,1,0:T(8,128)S(1)} %get-tuple-element.40, f32[2048]{0:T(1024)S(1)} %copy-done.11), kind=kOutput, calls=%fused_computation.4 | convolution fusion | flops 134512640 | bytes 8855552 | tf_op jit(solution)/shard_map/dot_general | solution.py:187
  226.3 0.7 copy.222
  228.3 3.9 %reduce-scatter.2.cloned.1.call-done = bf16[16,1024]{1,0:T(8,128)(2,1)} async-done(((bf16[16,2048]{1,0:T(8,128)(2,1)}), bf16[16,1024]{1,0:T(8,128)(2,1)}) %reduce-scatter.2.cloned.1.call-update) | async-done | bytes 32784 | tf_op jit(solution)/shard_map/reduce_scatter | solution.py:192
  232.2 1.4 reshape.170
  (99 shorter events, 7.0 us)
Async XLA Ops:
  7.2 38.9 %copy-start = (bf16[2048,64]{0,1:T(8,128)(2,1)S(1)}, bf16[2048,64]{0,1:T(8,128)(2,1)}, u32[]{:S(2)}) copy-start(bf16[2048,64]{0,1:T(8,128)(2,1)} %param.27) | copy-start | bytes 786436
  7.2 37.8 %copy-start.7 = (bf16[128,2048]{1,0:T(8,128)(2,1)S(1)}, bf16[128,2048]{1,0:T(8,128)(2,1)}, u32[]{:S(2)}) copy-start(bf16[128,2048]{1,0:T(8,128)(2,1)} %param.24) | copy-start | bytes 1572868
  7.2 38.8 %copy-start.17 = (s32[4]{0:T(128)S(1)}, s32[4]{0:T(128)}, u32[]{:S(2)}) copy-start(s32[4]{0:T(128)} %param.41) | copy-start | bytes 52
  7.2 38.8 %copy-start.16 = (f32[32]{0:T(128)S(1)}, f32[32]{0:T(128)}, u32[]{:S(2)}) copy-start(f32[32]{0:T(128)} %param.32) | copy-start | bytes 388
  7.2 39.0 %copy-start.14 = (f32[32]{0:T(128)S(1)}, f32[32]{0:T(128)}, u32[]{:S(2)}) copy-start(f32[32]{0:T(128)} %param.31) | copy-start | bytes 388
  7.2 39.0 %copy-start.10 = (bf16[4,4,32]{2,1,0:T(4,128)(2,1)S(1)}, bf16[4,4,32]{2,1,0:T(4,128)(2,1)}, u32[]{:S(2)}) copy-start(bf16[4,4,32]{2,1,0:T(4,128)(2,1)} %param.40) | copy-start | bytes 3076
  7.2 56.5 %copy-start.3 = (bf16[4,7,2048]{2,0,1:T(4,128)(2,1)S(1)}, bf16[4,7,2048]{2,0,1:T(4,128)(2,1)}, u32[]{:S(2)}) copy-start(bf16[4,7,2048]{2,0,1:T(4,128)(2,1)} %param.37) | copy-start | bytes 344068
  7.2 57.4 %copy-start.4 = (bf16[4,7,512]{2,0,1:T(4,128)(2,1)S(1)}, bf16[4,7,512]{2,0,1:T(4,128)(2,1)}, u32[]{:S(2)}) copy-start(bf16[4,7,512]{2,0,1:T(4,128)(2,1)} %param.38) | copy-start | bytes 86020
  7.3 58.3 %copy-start.5 = (bf16[4,7,512]{2,0,1:T(4,128)(2,1)S(1)}, bf16[4,7,512]{2,0,1:T(4,128)(2,1)}, u32[]{:S(2)}) copy-start(bf16[4,7,512]{2,0,1:T(4,128)(2,1)} %param.39) | copy-start | bytes 86020
  7.3 59.0 %copy-start.12 = (f32[4,512]{1,0:T(4,128)S(1)}, f32[4,512]{1,0:T(4,128)}, u32[]{:S(2)}) copy-start(f32[4,512]{1,0:T(4,128)} %param.29) | copy-start | bytes 24580
  7.3 59.1 %copy-start.8 = (f32[4,2048]{1,0:T(4,128)S(1)}, f32[4,2048]{1,0:T(4,128)}, u32[]{:S(2)}) copy-start(f32[4,2048]{1,0:T(4,128)} %param.28) | copy-start | bytes 98308
  7.3 73.1 %all-gather.3.cloned.1.call-start = ((), (), s32[]{:S(2)}) async-start(), calls=%async_computation.6 | async-start | bytes 1114112 | tf_op jit(solution)/shard_map/all_gather | solution.py:150
  11.3 34.8 %copy-start.6 = (bf16[16,2048]{1,0:T(8,128)(2,1)S(1)}, bf16[16,2048]{1,0:T(8,128)(2,1)}, u32[]{:S(2)}) copy-start(bf16[16,2048]{1,0:T(8,128)(2,1)} %reshape.162) | copy-start | bytes 196612
  11.3 209.8 %all-gather.5.cloned.1.call-start = ((), (), s32[]{:S(2)}) async-start(), calls=%async_computation.7 | async-start | bytes 8912896 | tf_op jit(solution)/shard_map/all_gather | solution.py:189
  13.7 16.4 %all-to-all-start.2 = ((bf16[128,16,32]{0,2,1:T(8,128)(2,1)}), bf16[128,16,32]{0,2,1:T(8,128)(2,1)S(1)}, u32[]{:S(2)}, u32[]{:S(2)}) async-start(bf16[128,16,32]{0,2,1:T(8,128)(2,1)} %bitcast.19), calls=%async_computation.2 | async-start | bytes 262144 | tf_op jit(solution)/shard_map/all_to_all | solution.py:144
  30.1 11.3 %all-to-all-start.3 = ((bf16[128,16,32]{0,2,1:T(8,128)(2,1)}), bf16[128,16,32]{0,2,1:T(8,128)(2,1)S(1)}, u32[]{:S(2)}, u32[]{:S(2)}) async-start(bf16[128,16,32]{0,2,1:T(8,128)(2,1)} %bitcast.22), calls=%async_computation.3 | async-start | bytes 262144 | tf_op jit(solution)/shard_map/all_to_all | solution.py:145
  41.4 18.3 %all-to-all-start = ((bf16[128,16,128]{0,2,1:T(8,128)(2,1)}), bf16[128,16,128]{0,2,1:T(8,128)(2,1)S(1)}, u32[]{:S(2)}, u32[]{:S(2)}) async-start(bf16[128,16,128]{0,2,1:T(8,128)(2,1)} %bitcast.13), calls=%async_computation | async-start | bytes 1048576 | tf_op jit(solution)/shard_map/all_to_all | solution.py:142
  46.2 36.4 %copy-start.9 = (bf16[16,32]{1,0:T(8,128)(2,1)}, bf16[16,32]{1,0:T(8,128)(2,1)S(1)}, u32[]{:S(2)}) copy-start(bf16[16,32]{1,0:T(8,128)(2,1)S(1)} %convolution_convert_fusion.1) | copy-start | bytes 3076
  59.6 20.4 %all-to-all-start.1 = ((bf16[128,16,128]{0,2,1:T(8,128)(2,1)}), bf16[128,16,128]{0,2,1:T(8,128)(2,1)S(1)}, u32[]{:S(2)}, u32[]{:S(2)}) async-start(bf16[128,16,128]{0,2,1:T(8,128)(2,1)} %bitcast.16), calls=%async_computation.1 | async-start | bytes 1048576 | tf_op jit(solution)/shard_map/all_to_all | solution.py:143
  80.0 8.5 %copy-start.13 = (f32[4,512]{1,0:T(4,128)S(1)}, f32[4,512]{1,0:T(4,128)}, u32[]{:S(2)}) copy-start(f32[4,512]{1,0:T(4,128)} %param.30) | copy-start | bytes 24580
  83.5 13.0 %all-to-all-start.4 = ((bf16[16,16,320]{2,1,0:T(8,128)(2,1)}), bf16[16,16,320]{2,1,0:T(8,128)(2,1)S(1)}, u32[]{:S(2)}, u32[]{:S(2)}) async-start(bf16[16,16,320]{2,1,0:T(8,128)(2,1)} %bitcast.25), calls=%async_computation.4 | async-start | bytes 393216 | tf_op jit(solution)/shard_map/all_to_all | solution.py:152
  88.3 143.9 %reduce-scatter.2.cloned.1.call-start = ((), (), s32[]{:S(2)}) async-start(), calls=%async_computation.8 | async-start | bytes 98304 | tf_op jit(solution)/shard_map/reduce_scatter | solution.py:192
  97.9 2.7 %copy-start.2 = (f32[4,32,64,128]{3,2,1,0:T(8,128)S(1)}, f32[4,32,64,128]{3,2,1,0:T(8,128)}, u32[]{:S(2)}) copy-start(f32[4,32,64,128]{3,2,1,0:T(8,128)} %param.36) | copy-start | bytes 12582916
  108.2 2.0 copy-start.1
  110.2 6.8 %copy-start.15 = (f32[32]{0:T(128)S(1)}, f32[32]{0:T(128)}, u32[]{:S(2)}) copy-start(f32[32]{0:T(128)} %param.33) | copy-start | bytes 388
  110.2 110.8 %copy-start.11 = (f32[2048]{0:T(1024)S(1)}, f32[2048]{0:T(1024)}, u32[]{:S(2)}) copy-start(f32[2048]{0:T(1024)} %param.34) | copy-start | bytes 24580
Sparse Core Ops, SparseCore 0:
  11.4 63.3 all-gather.2
  77.5 143.4 all-gather.4
  226.4 5.7 reduce-scatter.1
where the time goes:
time: 241 us; the launch traced here: 240 us
  waiting for transfers between devices  154 us (64%)
  matrix products  24.4 us (10%)
  starting transfers between devices  24.3 us (10%)
  local copies, waits for them, and re-layouts  18.5 us (8%)
  between operations  14.2 us (6%)
    all_gather x1, waiting for transfers between devices, on_device(): lax.all_gather(out_weight, 'kv', axis=1, tiled=True)  103 us
    all_to_all x1, waiting for transfers between devices, on_device(): lax.all_to_all(gate_weight, 'kv', split_axis=1, concat_axis=0, tiled=True)  13.3 us
    all_to_all x1, waiting for transfers between devices, on_device(): lax.all_to_all(value_weight, 'kv', split_axis=1, concat_axis=0, tiled=True)  12.8 us
    unnamed x45, local copies, waits for them, and re-layouts  10.6 us
    all_to_all x1, starting transfers between devices, on_device(): lax.all_to_all(write_weight, 'kv', split_axis=1, concat_axis=0, tiled=True)  8.2 us
    all_to_all x1, waiting for transfers between devices, on_device(): lax.all_to_all(everyone, 'kv', split_axis=0, concat_axis=1, tiled=True)  7.89 us
    dot_general x1, matrix products, advance(): jnp.einsum('sh,shp,shn->hpn', weight_now, prev_x, prev_b, precision=highest)  7.61 us
    dot_general x1, matrix products, advance(): jnp.einsum('thn,hpn->thp', cur_c, root, precision=highest)  6.79 us
  transfers between devices with their start and end apart: 8, of which 7 were waited for; matrix products, arithmetic and copies ran while one was open for 15% of the time, Pallas kernels for 0%

commit v1 on v0

--- a/solution.py
+++ b/solution.py
@@ -1,6 +1,10 @@
+import functools
+
 import jax
 import jax.numpy as jnp
 from jax import lax
+from jax.experimental import pallas as pl
+from jax.experimental.pallas import tpu as pltpu
 from jax.sharding import PartitionSpec as P
 
 STATE_DIM = 128
@@ -100,6 +104,316 @@
     grouped = grouped * lax.rsqrt(jnp.mean(grouped * grouped, axis=-1, keepdims=True) + EPSILON)
     result = (grouped.reshape(proposals, -1) * output_gain).astype(jnp.bfloat16)
     return (result, root, window_x, window_b, window_c)
+
+
+MESH = pl.DeviceIdType.MESH
+
+
+def near_split(count):
+    low = max(d for d in range(1, count + 1) if count % d == 0 and d * d <= count)
+    return count // low, low
+
+
+def remote(src, dst, send, recv, kv, tp):
+    return pltpu.make_async_remote_copy(
+        src_ref=src,
+        dst_ref=dst,
+        send_sem=send,
+        recv_sem=recv,
+        device_id={"kv": kv, "tp": tp},
+        device_id_type=MESH,
+    )
+
+
+class Gather:
+    def __init__(self, own, slots, send, recv, n_kv):
+        self.own, self.slots, self.send, self.recv = own, slots, send, recv
+        self.far, self.near = near_split(n_kv)
+        self.me, self.tp = lax.axis_index("kv"), lax.axis_index("tp")
+        self.h, self.l = lax.div(self.me, self.near), lax.rem(self.me, self.near)
+        self.copies = []
+
+    def start(self, src, block, kv):
+        copy = remote(
+            src,
+            self.slots.at[block],
+            self.send.at[len(self.copies)],
+            self.recv.at[block],
+            kv,
+            self.tp,
+        )
+        copy.start()
+        self.copies.append(copy)
+
+    def arrive(self, block):
+        remote(
+            self.own, self.slots.at[block], self.send.at[0], self.recv.at[block], self.me, self.tp
+        ).wait_recv()
+
+    def first(self):
+        for step in range(1, self.far):
+            self.start(self.own, self.me, lax.rem(self.h + step, self.far) * self.near + self.l)
+        for step in range(1, self.near):
+            self.start(self.own, self.me, self.h * self.near + lax.rem(self.l + step, self.near))
+
+    def relay(self):
+        for step in range(1, self.far):
+            block = lax.rem(self.h + self.far - step, self.far) * self.near + self.l
+            self.arrive(block)
+            for side in range(1, self.near):
+                self.start(
+                    self.slots.at[block],
+                    block,
+                    self.h * self.near + lax.rem(self.l + side, self.near),
+                )
+
+    def finish(self):
+        for side in range(1, self.near):
+            l = lax.rem(self.l + self.near - side, self.near)
+            for step in range(self.far):
+                self.arrive(lax.rem(self.h + self.far - step, self.far) * self.near + l)
+
+    def drain(self):
+        for copy in self.copies:
+            copy.wait_send()
+
+
+def project_kernel(
+    n_kv, n_tp, x_ref, wide_ref, thin_ref, out_ref,
+    xs, wides, thins, mine, back,
+    x_send, x_recv, tp_send, tp_recv, wide_send, wide_recv, thin_send, thin_recv,
+    back_send, back_recv, local_sem,
+):
+    me, tp = lax.axis_index("kv"), lax.axis_index("tp")
+    barrier = pltpu.get_barrier_semaphore()
+    for step in range(1, n_kv):
+        pl.semaphore_signal(
+            barrier, inc=1, device_id={"kv": lax.rem(me + step, n_kv), "tp": tp}, device_id_type=MESH
+        )
+    for step in range(1, n_tp):
+        pl.semaphore_signal(
+            barrier, inc=1, device_id={"kv": me, "tp": lax.rem(tp + step, n_tp)}, device_id_type=MESH
+        )
+    own = [
+        pltpu.make_async_copy(x_ref, xs.at[tp, me], local_sem.at[0]),
+        pltpu.make_async_copy(wide_ref.at[me], wides.at[me], local_sem.at[1]),
+        pltpu.make_async_copy(thin_ref.at[me], thins.at[me], local_sem.at[2]),
+    ]
+    for copy in own:
+        copy.start()
+    pl.semaphore_wait(barrier, n_kv - 1 + n_tp - 1)
+
+    gather = Gather(x_ref, xs.at[tp], x_send, x_recv, n_kv)
+    gather.first()
+    sends = []
+
+    def send_weights(lo, hi):
+        for step in range(lo, hi):
+            peer = lax.rem(me + step, n_kv)
+            for src, dst, ss, rs in (
+                (wide_ref, wides, wide_send, wide_recv),
+                (thin_ref, thins, thin_send, thin_recv),
+            ):
+                copy = remote(src.at[peer], dst.at[me], ss.at[step - 1], rs.at[step - 1], peer, tp)
+                copy.start()
+                sends.append(copy)
+
+    cut = 1 + n_kv // 4
+    send_weights(1, cut)
+    gather.relay()
+    send_weights(cut, n_kv)
+    gather.finish()
+    for copy in own:
+        copy.wait()
+    shares = []
+    for step in range(1, n_tp):
+        copy = remote(
+            xs.at[tp], xs.at[tp], tp_send.at[step - 1], tp_recv.at[step - 1],
+            me, lax.rem(tp + step, n_tp),
+        )
+        copy.start()
+        shares.append(copy)
+    for copy in shares:
+        copy.wait_recv()
+    for copy in sends:
+        copy.wait_recv()
+
+    tokens = x_ref.shape[0]
+    half = x_ref.shape[1]
+    depth = wide_ref.shape[1]
+    per = n_kv // n_tp
+    wide_sum = None
+    thin_sum = None
+    for t in range(n_tp):
+        rows = xs[t].reshape(n_kv * tokens, half)
+        block = wides[t * per : (t + 1) * per].reshape(half, wide_ref.shape[2])
+        term = jnp.dot(rows, block, preferred_element_type=jnp.float32)
+        wide_sum = term if wide_sum is None else wide_sum + term
+        for k in range(per):
+            term = lax.dot_general(
+                rows[:, k * depth : (k + 1) * depth],
+                thins[t * per + k],
+                (((1,), (1,)), ((), ())),
+                preferred_element_type=jnp.float32,
+            )
+            thin_sum = term if thin_sum is None else thin_sum + term
+    wide_cols = wide_ref.shape[2]
+    cols = mine.shape[2]
+    mine[:, :, 0:wide_cols] = wide_sum.astype(jnp.bfloat16).reshape(n_kv, tokens, wide_cols)
+    mine[:, :, wide_cols:cols] = thin_sum.astype(jnp.bfloat16).reshape(
+        n_kv, tokens, cols - wide_cols
+    )
+    returns = []
+    for step in range(1, n_kv):
+        peer = lax.rem(me + step, n_kv)
+        copy = remote(
+            mine.at[peer], back.at[me], back_send.at[step - 1], back_recv.at[step - 1], peer, tp
+        )
+        copy.start()
+        returns.append(copy)
+    out_ref[me] = mine[me]
+    gather.drain()
+    for copy in shares + sends:
+        copy.wait_send()
+    for step, copy in enumerate(returns, 1):
+        copy.wait_recv()
+        source = lax.rem(me + n_kv - step, n_kv)
+        out_ref[source] = back[source]
+    for copy in returns:
+        copy.wait_send()
+
+
+def project(x, wide, thin, n_kv, n_tp):
+    tokens, half = x.shape
+    cols = wide.shape[2] + thin.shape[1]
+    dma = pltpu.SemaphoreType.DMA
+    far, near = near_split(n_kv)
+    count = far - 1 + (near - 1) * far
+    peers = (max(n_kv - 1, 1),)
+    return pl.pallas_call(
+        functools.partial(project_kernel, n_kv, n_tp),
+        out_shape=jax.ShapeDtypeStruct((n_kv, tokens, cols), jnp.bfloat16),
+        in_specs=[pl.BlockSpec(memory_space=pltpu.VMEM)] * 3,
+        out_specs=pl.BlockSpec(memory_space=pltpu.VMEM),
+        scratch_shapes=[
+            pltpu.VMEM((n_tp, n_kv, tokens, half), jnp.bfloat16),
+            pltpu.VMEM(wide.shape, jnp.bfloat16),
+            pltpu.VMEM(thin.shape, jnp.bfloat16),
+            pltpu.VMEM((n_kv, tokens, cols), jnp.bfloat16),
+            pltpu.VMEM((n_kv, tokens, cols), jnp.bfloat16),
+            dma((count,)), dma((n_kv,)), dma((max(n_tp - 1, 1),)), dma((max(n_tp - 1, 1),)),
+            dma(peers), dma(peers), dma(peers), dma(peers), dma(peers), dma(peers), dma((3,)),
+        ],
+        compiler_params=pltpu.CompilerParams(collective_id=0, has_side_effects=True),
+        name="project",
+    )(x, wide, thin)
+
+
+def mix_kernel(
+    n_kv, n_tp, y_ref, w_ref, out_ref,
+    ys, mine, parts, y_send, y_recv, part_send, part_recv, local_sem,
+):
+    me, tp = lax.axis_index("kv"), lax.axis_index("tp")
+    total = n_kv * n_tp
+    flat = me * n_tp + tp
+    barrier = pltpu.get_barrier_semaphore()
+
+    def greet(step, carry):
+        other = lax.rem(flat + step, total)
+        pl.semaphore_signal(
+            barrier,
+            inc=1,
+            device_id={"kv": lax.div(other, n_tp), "tp": lax.rem(other, n_tp)},
+            device_id_type=MESH,
+        )
+        return carry
+
+    lax.fori_loop(1, total, greet, 0)
+    own = pltpu.make_async_copy(y_ref, ys.at[me], local_sem.at[0])
+    own.start()
+    pl.semaphore_wait(barrier, total - 1)
+    gather = Gather(y_ref, ys, y_send, y_recv, n_kv)
+    gather.first()
+    gather.relay()
+    own.wait()
+    gather.finish()
+
+    tokens, cols = y_ref.shape[0], w_ref.shape[1]
+    product = jnp.dot(
+        ys[...].reshape(n_kv * tokens, y_ref.shape[1]),
+        w_ref[...],
+        preferred_element_type=jnp.float32,
+    )
+    mine[...] = product.astype(jnp.bfloat16).reshape(n_kv, tokens, cols)
+    per = n_kv // n_tp
+    side, place = lax.div(me, per), lax.rem(me, per)
+
+    def part(step):
+        return remote(
+            mine.at[lax.rem(me + step, n_kv)],
+            parts.at[tp, place],
+            part_send.at[step],
+            part_recv.at[tp, place],
+            lax.rem(me + step, n_kv),
+            side,
+        )
+
+    for step in range(1, n_kv):
+        part(step).start()
+
+    @pl.when(side != tp)
+    def _():
+        part(0).start()
+
+    @pl.when(side == tp)
+    def _():
+        parts[tp, place] = mine[me]
+
+    gather.drain()
+    for t in range(n_tp):
+        for k in range(per):
+            incoming = remote(
+                mine.at[0], parts.at[t, k], part_send.at[0], part_recv.at[t, k], me, tp
+            )
+
+            @pl.when(jnp.logical_or(t != tp, tp * per + k != me))
+            def _():
+                incoming.wait_recv()
+
+    for k in range(per):
+        value = parts[0, k].astype(jnp.float32)
+        for t in range(1, n_tp):
+            value = value + parts[t, k].astype(jnp.float32)
+        out_ref[:, k * cols : (k + 1) * cols] = value.astype(jnp.bfloat16)
+    for step in range(1, n_kv):
+        part(step).wait_send()
+
+    @pl.when(side != tp)
+    def _():
+        part(0).wait_send()
+
+
+def mix(y, weight, n_kv, n_tp):
+    tokens, depth = y.shape
+    cols = weight.shape[1]
+    dma = pltpu.SemaphoreType.DMA
+    far, near = near_split(n_kv)
+    count = far - 1 + (near - 1) * far
+    per = n_kv // n_tp
+    return pl.pallas_call(
+        functools.partial(mix_kernel, n_kv, n_tp),
+        out_shape=jax.ShapeDtypeStruct((tokens, per * cols), jnp.bfloat16),
+        in_specs=[pl.BlockSpec(memory_space=pltpu.VMEM)] * 2,
+        out_specs=pl.BlockSpec(memory_space=pltpu.VMEM),
+        scratch_shapes=[
+            pltpu.VMEM((n_kv, tokens, depth), jnp.bfloat16),
+            pltpu.VMEM((n_kv, tokens, cols), jnp.bfloat16),
+            pltpu.VMEM((n_tp, per, tokens, cols), jnp.bfloat16),
+            dma((count,)), dma((n_kv,)), dma((n_kv,)), dma((n_tp, per)), dma((1,)),
+        ],
+        compiler_params=pltpu.CompilerParams(collective_id=1, has_side_effects=True),
+        name="mix",
+    )(y, weight)
 
 
 def on_device(
@@ -138,20 +452,18 @@
         step_weight, lax.axis_index("tp") * head_count, head_count, 1
     )
     step_now = jnp.dot(flat, own_step, preferred_element_type=jnp.float32).astype(jnp.bfloat16)
-    slabs = (
-        lax.all_to_all(gate_weight, "kv", split_axis=1, concat_axis=0, tiled=True),
-        lax.all_to_all(value_weight, "kv", split_axis=1, concat_axis=0, tiled=True),
-        lax.all_to_all(write_weight, "kv", split_axis=1, concat_axis=0, tiled=True),
-        lax.all_to_all(read_weight, "kv", split_axis=1, concat_axis=0, tiled=True),
-    )
-    spans = [slab.shape[1] for slab in slabs]
-    narrow = jnp.concatenate(slabs, axis=1)
-    everyone = jnp.dot(
-        lax.all_gather(flat, "kv", axis=0, tiled=True), narrow, preferred_element_type=jnp.float32
-    ).astype(jnp.bfloat16)
-    returned = lax.all_to_all(everyone, "kv", split_axis=0, concat_axis=1, tiled=True)
-    ranks = lax.axis_size("kv")
-    returned = returned.reshape(token_count, ranks, sum(spans))
+    ranks, n_tp = lax.axis_size("kv"), lax.axis_size("tp")
+    depth = gate_weight.shape[0]
+    cut = [
+        item.reshape(depth, ranks, item.shape[1] // ranks)
+        for item in (gate_weight, value_weight, write_weight, read_weight)
+    ]
+    spans = [item.shape[2] for item in cut]
+    wide = jnp.concatenate(cut[:2], axis=2).transpose(1, 0, 2)
+    thin = jnp.concatenate(cut[2:], axis=2).transpose(1, 2, 0)
+    half = width // n_tp
+    own_features = lax.dynamic_slice_in_dim(flat, lax.axis_index("tp") * half, half, 1)
+    returned = project(own_features, wide, thin, ranks, n_tp).transpose(1, 0, 2)
     pieces_out = []
     offset = 0
     for span in spans:
@@ -184,15 +496,8 @@
         output_gain,
     )
     flat_y = normal_out.reshape(token_count, -1)
-    partial_sum = jnp.dot(
-        flat_y,
-        lax.all_gather(out_weight, "kv", axis=1, tiled=True),
-        preferred_element_type=jnp.float32,
-    )
-    summed = lax.psum_scatter(
-        partial_sum.astype(jnp.bfloat16), "tp", scatter_dimension=1, tiled=True
-    ).astype(jnp.float32)
-    mixed = summed.astype(jnp.bfloat16).reshape(seq_local, proposals, summed.shape[1])
+    mixed = mix(flat_y, out_weight, ranks, n_tp)
+    mixed = mixed.reshape(seq_local, proposals, mixed.shape[1])
     return (mixed, root_state, next_value, next_write, next_read, shaped[4])
 
 

time: 241 us -> 120 us (0.50)
  waiting for transfers between devices: 154 us -> 0 us
  Pallas kernels: 0 us -> 77.6 us
  starting transfers between devices: 24.3 us -> 0 us
  between operations: 14.2 us -> 1.15 us
  local copies, waits for them, and re-layouts: 18.5 us -> 11.6 us
  other arithmetic: 2.3 us -> 5.76 us
  matrix products: 24.4 us -> 21.4 us
    all_gather x2 -> x0, waiting for transfers between devices: 103 us -> none  [the longest x1 103 us: on_device(): lax.all_gather(out_weight, 'kv', axis=1, tiled=True)]
    pallas_call x0 -> x2, Pallas kernels: none -> 77.6 us  [the longest x1 55 us: project(): pl.pallas_call(functools.partial(project_kernel, n_kv, n_tp), out_shape=j...]
    all_to_all x5 -> x0, waiting for transfers between devices: 46.2 us -> none  [the longest x1 13.3 us: on_device(): lax.all_to_all(gate_weight, 'kv', split_axis=1, concat_axis=0, tiled=True)]
    all_to_all x5 -> x0, starting transfers between devices: 24 us -> none  [the longest x1 8.2 us: on_device(): lax.all_to_all(write_weight, 'kv', split_axis=1, concat_axis=0, tiled=True)]
    dot_general x2 -> x0, matrix products: 7.52 us -> none  [the longest x1 5.22 us: on_device(): jnp.dot(flat_y, lax.all_gather(out_weight, 'kv', axis=1, tiled=True), pre...]
    unnamed x45 -> x43, local copies, waits for them, and re-layouts: 10.6 us -> 5.09 us
    reduce_scatter x1 -> x0, waiting for transfers between devices: 3.88 us -> none  [on_device(): lax.psum_scatter(partial_sum.astype(jnp.bfloat16), 'tp', scatter_dimensio...]
    dot_general x1, matrix products: 7.61 us -> 10.4 us  [advance(): jnp.einsum('sh,shp,shn->hpn', weight_now, prev_x, prev_b, precision=highest)]
  transfers between devices with their start and end apart: 8 -> 0, of which waited for: 7 -> 0; matrix products, arithmetic and copies ran while one was open for 15% -> 0% of each run, Pallas kernels for 0% -> 0%
where the time goes in v1:
time: 120 us
  Pallas kernels  77.6 us (65%)
  matrix products  21.4 us (18%)
  local copies, waits for them, and re-layouts  11.6 us (10%)
  other arithmetic  5.76 us (5%)
  blocking collectives  2.34 us (2%)
    pallas_call x1, Pallas kernels, project(): pl.pallas_call(functools.partial(project_kernel, n_kv, n_tp), out_shape=j...  55 us
    pallas_call x1, Pallas kernels, mix(): pl.pallas_call(functools.partial(mix_kernel, n_kv, n_tp), out_shape=jax.S...  22.7 us
    dot_general x1, matrix products, advance(): jnp.einsum('sh,shp,shn->hpn', weight_now, prev_x, prev_b, precision=highest)  10.4 us
    dot_general x1, matrix products, advance(): jnp.einsum('thn,hpn->thp', cur_c, root, precision=highest)  8.47 us
    unnamed x43, local copies, waits for them, and re-layouts  5.09 us

profile of v1, /device:TPU:0, one launch (start us, length us, event | category | flops | bytes accessed | tf_op | source)
XLA Modules:
  0.0 119.8 jit_solution(17075383605704767689)
XLA Ops:
  0.7 2.3 %all_gather.3 = bf16[4,4,2048]{2,1,0:T(4,128)(2,1)S(1)} all-gather(bf16[4,4,1024]{2,1,0:T(4,128)(2,1)} %param.21), channel_id=1, replica_groups=mesh['kv'=16,'tp'=2] {'tp'}, dimensions={2}, use_global_device_ids=true | all-gather | bytes 98304 | tf_op jit(solution)/shard_map/all_gather | solution.py:442
  3.0 0.1 fusion.5
  3.1 0.8 fusion.7
  4.0 0.6 constant_dynamic-slice_fusion.x_ref
  4.6 1.3 %copy.146 = bf16[128,2048]{0,1:T(8,128)(2,1)S(1)} copy(bf16[128,2048]{1,0:T(8,128)(2,1)} %param.23) | data formatting | bytes 1048576 | tf_op args[2]
  5.9 0.3 copy.148
  6.2 1.3 %copy.147 = bf16[128,2048]{0,1:T(8,128)(2,1)S(1)} copy(bf16[128,2048]{1,0:T(8,128)(2,1)} %param.24) | data formatting | bytes 1048576 | tf_op args[3]
  7.6 0.3 copy.149
  7.9 1.1 maximum_bitcast_fusion.wide_ref
  9.0 0.1 copy.150
  9.3 0.7 maximum_bitcast_fusion.1.thin_ref
  10.0 55.0 %project.1 = bf16[16,16,320]{2,1,0:T(8,128)(2,1)} custom-call(bf16[16,1024]{1,0:T(8,128)(2,1)} %constant_dynamic-slice_fusion.x_ref, bf16[16,128,256]{2,1,0:T(8,128)(2,1)} %maximum_bitcast_fusion.wide_ref, bf16[16,64,128]{2,1,0:T(8,128)(2,1)} %maximum_bitcast_fusion.1.thin_ref), custom_call_target="tpu_custom_call" | custom-call | tf_op jit(solution)/shard_map/project/pallas_call | solution.py:293
  65.0 0.9 fusion.35
  66.0 0.8 gather_fusion.1
  66.9 0.1 pad_maximum_fusion
  67.1 0.3 divide_multiply_fusion.1
  67.4 0.2 reshape.154
  67.8 0.6 gather_fusion.2
  68.7 0.1 convolution_convert_fusion
  69.3 10.4 %multiply_add_fusion = f32[4,32,64,128]{3,2,1,0:T(8,128)} fusion(f32[4,32,64,128]{3,2,1,0:T(8,128)} %param.36, f32[4,4,32,128]{3,1,2,0:T(4,128)S(1)} %bitcast.94, f32[4,32]{1,0:T(4,128)S(1)} %exp.62, f32[4,4,32,64]{3,2,1,0:T(8,128)S(1)} %reshape.154, f32[4,4,32]{1,2,0:T(8,128)S(1)} %copy.141), kind=kOutput, calls=%fused_computation.3 | convolution fusion | flops 52461568 | bytes 8784384 | tf_op jit(solution)/shard_map/vmap(sh,shp,shn->hpn)/dot_general | solution.py:66
  79.9 0.6 gather_fusion
  80.7 8.5 %fusion.51 = f32[4,32,64,4]{2,3,1,0:T(4,128)S(1)} fusion(f32[4,32,64,128]{3,2,1,0:T(8,128)} %multiply_add_fusion, f32[4,4,32,128]{3,1,2,0:T(4,128)S(1)} %bitcast.95), kind=kOutput, calls=%fused_computation.110 | convolution fusion | flops 50331648 | bytes 4587520 | tf_op jit(solution)/shard_map/vmap(thn,hpn->thp)/dot_general | solution.py:91
  89.5 1.1 fusion.1
  90.6 0.2 reshape.165
  90.8 1.2 %fusion.3 = f32[4,32,64,4]{2,3,1,0:T(4,128)S(1)} fusion(f32[4,4,4,32]{1,2,3,0:T(4,128)S(1)} %fusion.1, f32[4,4,32,64]{3,2,1,0:T(8,128)S(1)} %reshape.165), kind=kOutput, calls=%fused_computation.13 | convolution fusion | flops 1572864 | bytes 270336 | tf_op jit(solution)/shard_map/vmap(tsh,shp->thp)/dot_general | solution.py:100
  92.2 0.3 multiply_reduce_fusion
  93.1 0.7 fusion.22.y_ref
  93.8 22.7 %mix.1 = bf16[16,1024]{1,0:T(8,128)(2,1)} custom-call(bf16[16,2048]{1,0:T(8,128)(2,1)} %fusion.22.y_ref, bf16[2048,128]{1,0:T(8,128)(2,1)} %w_ref.1), custom_call_target="tpu_custom_call" | custom-call | tf_op jit(solution)/shard_map/mix/pallas_call | solution.py:403
  116.5 1.4 %reshape.169 = bf16[4,4,1024]{2,1,0:T(4,128)(2,1)} reshape(bf16[16,1024]{1,0:T(8,128)(2,1)} %mix.1) | data formatting | bytes 65536 | tf_op jit(solution)/shard_map/reshape | solution.py:500
  117.9 0.7 copy.171
  118.6 0.6 copy.172
  119.2 0.6 copy.173
  (79 shorter events, 2.4 us)
Async XLA Ops:
  0.6 68.1 %copy-start = (bf16[2048,64]{0,1:T(8,128)(2,1)S(1)}, bf16[2048,64]{0,1:T(8,128)(2,1)}, u32[]{:S(2)}) copy-start(bf16[2048,64]{0,1:T(8,128)(2,1)} %param.27) | copy-start | bytes 786436
  0.6 8.4 %copy-start.5 = (bf16[128,512]{1,0:T(8,128)(2,1)S(1)}, bf16[128,512]{1,0:T(8,128)(2,1)}, u32[]{:S(2)}) copy-start(bf16[128,512]{1,0:T(8,128)(2,1)} %param.25) | copy-start | bytes 393220
  0.7 8.5 %copy-start.6 = (bf16[128,512]{1,0:T(8,128)(2,1)S(1)}, bf16[128,512]{1,0:T(8,128)(2,1)}, u32[]{:S(2)}) copy-start(bf16[128,512]{1,0:T(8,128)(2,1)} %param.26) | copy-start | bytes 393220
  5.9 60.1 %copy-start.15 = (s32[4]{0:T(128)S(1)}, s32[4]{0:T(128)}, u32[]{:S(2)}) copy-start(s32[4]{0:T(128)} %param.41) | copy-start | bytes 52
  5.9 60.1 %copy-start.1 = (bf16[4,7,2048]{2,0,1:T(4,128)(2,1)S(1)}, bf16[4,7,2048]{2,0,1:T(4,128)(2,1)}, u32[]{:S(2)}) copy-start(bf16[4,7,2048]{2,0,1:T(4,128)(2,1)} %param.37) | copy-start | bytes 344068
  7.6 59.5 %copy-start.7 = (f32[4,2048]{1,0:T(4,128)S(1)}, f32[4,2048]{1,0:T(4,128)}, u32[]{:S(2)}) copy-start(f32[4,2048]{1,0:T(4,128)} %param.28) | copy-start | bytes 98308
  7.9 60.0 %copy-start.3 = (bf16[4,7,512]{2,0,1:T(4,128)(2,1)S(1)}, bf16[4,7,512]{2,0,1:T(4,128)(2,1)}, u32[]{:S(2)}) copy-start(bf16[4,7,512]{2,0,1:T(4,128)(2,1)} %param.38) | copy-start | bytes 86020
  9.0 59.5 %copy-start.11 = (f32[4,512]{1,0:T(4,128)S(1)}, f32[4,512]{1,0:T(4,128)}, u32[]{:S(2)}) copy-start(f32[4,512]{1,0:T(4,128)} %param.29) | copy-start | bytes 24580
  9.0 59.9 %copy-start.16 = (f32[32]{0:T(128)S(1)}, f32[32]{0:T(128)}, u32[]{:S(2)}) copy-start(f32[32]{0:T(128)} %param.32) | copy-start | bytes 388
  9.0 60.0 %copy-start.9 = (bf16[4,4,32]{2,1,0:T(4,128)(2,1)S(1)}, bf16[4,4,32]{2,1,0:T(4,128)(2,1)}, u32[]{:S(2)}) copy-start(bf16[4,4,32]{2,1,0:T(4,128)(2,1)} %param.40) | copy-start | bytes 3076
  9.0 60.0 %copy-start.13 = (f32[32]{0:T(128)S(1)}, f32[32]{0:T(128)}, u32[]{:S(2)}) copy-start(f32[32]{0:T(128)} %param.31) | copy-start | bytes 388
  65.0 2.6 %copy-start.2 = (bf16[16,16,320]{2,1,0:T(8,128)(2,1)S(1)}, bf16[16,16,320]{2,1,0:T(8,128)(2,1)}, u32[]{:S(2)}) copy-start(bf16[16,16,320]{2,1,0:T(8,128)(2,1)} %project.1) | copy-start | bytes 491524
  68.9 10.9 %copy-start.8 = (bf16[16,32]{1,0:T(8,128)(2,1)}, bf16[16,32]{1,0:T(8,128)(2,1)S(1)}, u32[]{:S(2)}) copy-start(bf16[16,32]{1,0:T(8,128)(2,1)S(1)} %convolution_convert_fusion) | copy-start | bytes 3076
  69.3 10.6 %copy-start.4 = (bf16[4,7,512]{2,0,1:T(4,128)(2,1)S(1)}, bf16[4,7,512]{2,0,1:T(4,128)(2,1)}, u32[]{:S(2)}) copy-start(bf16[4,7,512]{2,0,1:T(4,128)(2,1)} %param.39) | copy-start | bytes 86020
  69.3 11.3 %copy-start.12 = (f32[4,512]{1,0:T(4,128)S(1)}, f32[4,512]{1,0:T(4,128)}, u32[]{:S(2)}) copy-start(f32[4,512]{1,0:T(4,128)} %param.30) | copy-start | bytes 24580
  80.7 11.5 %copy-start.14 = (f32[32]{0:T(128)S(1)}, f32[32]{0:T(128)}, u32[]{:S(2)}) copy-start(f32[32]{0:T(128)} %param.33) | copy-start | bytes 388
  89.2 3.9 %copy-start.10 = (f32[2048]{0:T(1024)S(1)}, f32[2048]{0:T(1024)}, u32[]{:S(2)}) copy-start(f32[2048]{0:T(1024)} %param.34) | copy-start | bytes 24580

commit v2 on v1

--- a/solution.py
+++ b/solution.py
@@ -43,7 +43,7 @@
     skip_gain,
     output_gain,
 ):
-    highest = lax.Precision.HIGHEST
+    highest = lax.Precision.DEFAULT
     proposals = value_now.shape[0]
     head_count = step_bias.shape[0]
     group_count = write_now.shape[1] // STATE_DIM

time: 120 us -> 109 us (0.908)
  matrix products: 21.4 us -> 10.1 us
    dot_general x1, matrix products: 8.47 us -> 3.37 us  [advance(): jnp.einsum('thn,hpn->thp', cur_c, root, precision=highest)]
    dot_general x1, matrix products: 10.4 us -> 5.77 us  [advance(): jnp.einsum('sh,shp,shn->hpn', weight_now, prev_x, prev_b, precision=highest)]
where the time goes in v2:
time: 109 us
  Pallas kernels  77.7 us (71%)
  local copies, waits for them, and re-layouts  11.6 us (11%)
  matrix products  10.1 us (9%)
  other arithmetic  5.76 us (5%)
  blocking collectives  2.34 us (2%)
  between operations  1.13 us (1%)
    pallas_call x1, Pallas kernels, project(): pl.pallas_call(functools.partial(project_kernel, n_kv, n_tp), out_shape=j...  55 us
    pallas_call x1, Pallas kernels, mix(): pl.pallas_call(functools.partial(mix_kernel, n_kv, n_tp), out_shape=jax.S...  22.7 us
    dot_general x1, matrix products, advance(): jnp.einsum('sh,shp,shn->hpn', weight_now, prev_x, prev_b, precision=highest)  5.77 us
    unnamed x43, local copies, waits for them, and re-layouts  5.09 us
    dot_general x1, matrix products, advance(): jnp.einsum('thn,hpn->thp', cur_c, root, precision=highest)  3.37 us
    all_gather x1, blocking collectives, on_device(): whole = lax.all_gather(tokens, 'tp', axis=2, tiled=True)  2.34 us

profile of v2, /device:TPU:0, one launch (start us, length us, event | category | flops | bytes accessed | tf_op | source)
XLA Modules:
  0.0 108.6 jit_solution(16907155390508896206)
XLA Ops:
  0.7 2.3 %all_gather.3 = bf16[4,4,2048]{2,1,0:T(4,128)(2,1)S(1)} all-gather(bf16[4,4,1024]{2,1,0:T(4,128)(2,1)} %param.21), channel_id=1, replica_groups=mesh['kv'=16,'tp'=2] {'tp'}, dimensions={2}, use_global_device_ids=true | all-gather | bytes 98304 | tf_op jit(solution)/shard_map/all_gather | solution.py:442
  3.0 0.1 fusion.9
  3.1 0.8 fusion.11
  4.0 0.6 constant_dynamic-slice_fusion.x_ref
  4.6 1.3 %copy.146 = bf16[128,2048]{0,1:T(8,128)(2,1)S(1)} copy(bf16[128,2048]{1,0:T(8,128)(2,1)} %param.23) | data formatting | bytes 1048576 | tf_op args[2]
  5.9 0.3 copy.148
  6.2 1.3 %copy.147 = bf16[128,2048]{0,1:T(8,128)(2,1)S(1)} copy(bf16[128,2048]{1,0:T(8,128)(2,1)} %param.24) | data formatting | bytes 1048576 | tf_op args[3]
  7.6 0.3 copy.149
  7.9 1.1 %maximum_bitcast_fusion.wide_ref = bf16[16,128,256]{2,1,0:T(8,128)(2,1)} fusion(bf16[128,16,128]{2,0,1:T(8,128)(2,1)S(1)} %copy.149, bf16[128,16,128]{2,0,1:T(8,128)(2,1)S(1)} %copy.148), kind=kLoop, calls=%fused_computation.9 | loop fusion | flops 2097152 | bytes 2097152 | tf_op jit(solution)/shard_map/transpose | solution.py:462
  9.0 0.1 copy.150
  9.2 0.1 copy.151
  9.3 0.7 maximum_bitcast_fusion.1.thin_ref
  10.0 55.0 %project.1 = bf16[16,16,320]{2,1,0:T(8,128)(2,1)} custom-call(bf16[16,1024]{1,0:T(8,128)(2,1)} %constant_dynamic-slice_fusion.x_ref, bf16[16,128,256]{2,1,0:T(8,128)(2,1)} %maximum_bitcast_fusion.wide_ref, bf16[16,64,128]{2,1,0:T(8,128)(2,1)} %maximum_bitcast_fusion.1.thin_ref), custom_call_target="tpu_custom_call" | custom-call | tf_op jit(solution)/shard_map/project/pallas_call | solution.py:293
  65.0 0.9 fusion.44
  66.0 0.8 gather_fusion.1
  66.9 0.1 pad_maximum_fusion
  67.1 0.3 divide_multiply_fusion.1
  67.4 0.2 reshape.154
  67.8 0.6 gather_fusion.2
  68.7 0.1 convolution_convert_fusion
  69.3 5.8 %multiply_add_fusion = f32[4,32,64,128]{3,2,1,0:T(8,128)} fusion(f32[4,32,64,128]{3,2,1,0:T(8,128)} %param.36, bf16[4,4,32,128]{3,1,2,0:T(4,128)(2,1)S(1)} %bitcast.95, f32[4,32]{1,0:T(4,128)S(1)} %exp.62, f32[4,4,32,64]{3,2,1,0:T(8,128)S(1)} %reshape.154, f32[4,4,32]{1,2,0:T(8,128)S(1)} %copy.141), kind=kOutput, calls=%fused_computation.3 | convolution fusion | flops 10518528 | bytes 8653312 | tf_op jit(solution)/shard_map/vmap(sh,shp,shn->hpn)/dot_general | solution.py:66
  75.2 0.6 gather_fusion
  76.1 3.4 %fusion.61 = f32[4,32,64,4]{2,3,1,0:T(4,128)S(1)} fusion(f32[4,32,64,128]{3,2,1,0:T(8,128)} %multiply_add_fusion, bf16[4,4,32,128]{3,1,2,0:T(4,128)(2,1)S(1)} %bitcast.96), kind=kOutput, calls=%fused_computation.120 | convolution fusion | flops 8388608 | bytes 4456448 | tf_op jit(solution)/shard_map/vmap(thn,hpn->thp)/dot_general | solution.py:91
  79.5 0.2 reshape.165
  80.0 0.8 fusion.2
  81.0 0.3 multiply_reduce_fusion
  81.8 0.7 fusion.30.y_ref
  82.5 22.7 %mix.1 = bf16[16,1024]{1,0:T(8,128)(2,1)} custom-call(bf16[16,2048]{1,0:T(8,128)(2,1)} %fusion.30.y_ref, bf16[2048,128]{1,0:T(8,128)(2,1)} %w_ref.1), custom_call_target="tpu_custom_call" | custom-call | tf_op jit(solution)/shard_map/mix/pallas_call | solution.py:403
  105.2 1.4 %reshape.169 = bf16[4,4,1024]{2,1,0:T(4,128)(2,1)} reshape(bf16[16,1024]{1,0:T(8,128)(2,1)} %mix.1) | data formatting | bytes 65536 | tf_op jit(solution)/shard_map/reshape | solution.py:500
  106.6 0.7 copy.171
  107.3 0.6 copy.172
  108.0 0.6 copy.173
  (78 shorter events, 2.3 us)
Async XLA Ops:
  0.6 68.1 %copy-start = (bf16[2048,64]{0,1:T(8,128)(2,1)S(1)}, bf16[2048,64]{0,1:T(8,128)(2,1)}, u32[]{:S(2)}) copy-start(bf16[2048,64]{0,1:T(8,128)(2,1)} %param.27) | copy-start | bytes 786436
  0.6 8.4 %copy-start.5 = (bf16[128,512]{1,0:T(8,128)(2,1)S(1)}, bf16[128,512]{1,0:T(8,128)(2,1)}, u32[]{:S(2)}) copy-start(bf16[128,512]{1,0:T(8,128)(2,1)} %param.25) | copy-start | bytes 393220
  0.7 8.5 %copy-start.6 = (bf16[128,512]{1,0:T(8,128)(2,1)S(1)}, bf16[128,512]{1,0:T(8,128)(2,1)}, u32[]{:S(2)}) copy-start(bf16[128,512]{1,0:T(8,128)(2,1)} %param.26) | copy-start | bytes 393220
  5.9 60.1 %copy-start.15 = (s32[4]{0:T(128)S(1)}, s32[4]{0:T(128)}, u32[]{:S(2)}) copy-start(s32[4]{0:T(128)} %param.41) | copy-start | bytes 52
  5.9 60.1 %copy-start.1 = (bf16[4,7,2048]{2,0,1:T(4,128)(2,1)S(1)}, bf16[4,7,2048]{2,0,1:T(4,128)(2,1)}, u32[]{:S(2)}) copy-start(bf16[4,7,2048]{2,0,1:T(4,128)(2,1)} %param.37) | copy-start | bytes 344068
  7.6 59.5 %copy-start.7 = (f32[4,2048]{1,0:T(4,128)S(1)}, f32[4,2048]{1,0:T(4,128)}, u32[]{:S(2)}) copy-start(f32[4,2048]{1,0:T(4,128)} %param.28) | copy-start | bytes 98308
  7.9 60.0 %copy-start.3 = (bf16[4,7,512]{2,0,1:T(4,128)(2,1)S(1)}, bf16[4,7,512]{2,0,1:T(4,128)(2,1)}, u32[]{:S(2)}) copy-start(bf16[4,7,512]{2,0,1:T(4,128)(2,1)} %param.38) | copy-start | bytes 86020
  9.0 59.5 %copy-start.11 = (f32[4,512]{1,0:T(4,128)S(1)}, f32[4,512]{1,0:T(4,128)}, u32[]{:S(2)}) copy-start(f32[4,512]{1,0:T(4,128)} %param.29) | copy-start | bytes 24580
  9.0 59.9 %copy-start.16 = (f32[32]{0:T(128)S(1)}, f32[32]{0:T(128)}, u32[]{:S(2)}) copy-start(f32[32]{0:T(128)} %param.32) | copy-start | bytes 388
  9.0 60.0 %copy-start.9 = (bf16[4,4,32]{2,1,0:T(4,128)(2,1)S(1)}, bf16[4,4,32]{2,1,0:T(4,128)(2,1)}, u32[]{:S(2)}) copy-start(bf16[4,4,32]{2,1,0:T(4,128)(2,1)} %param.40) | copy-start | bytes 3076
  9.0 60.0 %copy-start.13 = (f32[32]{0:T(128)S(1)}, f32[32]{0:T(128)}, u32[]{:S(2)}) copy-start(f32[32]{0:T(128)} %param.31) | copy-start | bytes 388
  65.0 2.6 %copy-start.2 = (bf16[16,16,320]{2,1,0:T(8,128)(2,1)S(1)}, bf16[16,16,320]{2,1,0:T(8,128)(2,1)}, u32[]{:S(2)}) copy-start(bf16[16,16,320]{2,1,0:T(8,128)(2,1)} %project.1) | copy-start | bytes 491524
  68.9 6.2 %copy-start.8 = (bf16[16,32]{1,0:T(8,128)(2,1)}, bf16[16,32]{1,0:T(8,128)(2,1)S(1)}, u32[]{:S(2)}) copy-start(bf16[16,32]{1,0:T(8,128)(2,1)S(1)} %convolution_convert_fusion) | copy-start | bytes 3076
  69.3 5.9 %copy-start.4 = (bf16[4,7,512]{2,0,1:T(4,128)(2,1)S(1)}, bf16[4,7,512]{2,0,1:T(4,128)(2,1)}, u32[]{:S(2)}) copy-start(bf16[4,7,512]{2,0,1:T(4,128)(2,1)} %param.39) | copy-start | bytes 86020
  69.3 6.6 %copy-start.12 = (f32[4,512]{1,0:T(4,128)S(1)}, f32[4,512]{1,0:T(4,128)}, u32[]{:S(2)}) copy-start(f32[4,512]{1,0:T(4,128)} %param.30) | copy-start | bytes 24580
  76.0 4.9 %copy-start.14 = (f32[32]{0:T(128)S(1)}, f32[32]{0:T(128)}, u32[]{:S(2)}) copy-start(f32[32]{0:T(128)} %param.33) | copy-start | bytes 388
  76.1 5.7 %copy-start.10 = (f32[2048]{0:T(1024)S(1)}, f32[2048]{0:T(1024)}, u32[]{:S(2)}) copy-start(f32[2048]{0:T(1024)} %param.34) | copy-start | bytes 24580
